TPU v7x, 32 devices: a whole 2x2x4 slice. The times are simulated.
32 devices in a mesh: kv: 8 (over z, y), tp: 4 (over x, core).
Axes of the slice: x: 2, y: 2, z: 4, core: 2. Of those that a mesh axis runs over, the one named last changes fastest.
Arguments:
- tokens: bfloat16 [256, 4, 2048], P(None, None, ('kv', 'tp')), may hold values from -520 to 520
- input_norm_gain: bfloat16 [2048], replicated, may hold values from 0.099609375 to 1.8984375
- query_weight: bfloat16 [2048, 2048], P(None, 'kv'), may hold values from -0.125 to 0.125
- key_weight: bfloat16 [2048, 2048], P(None, 'kv'), may hold values from -0.125 to 0.125
- value_weight: bfloat16 [2048, 16, 128], P(None, 'kv', 'tp'), may hold values from -1.14904852 to 1.14904852
- output_gate_weight: bfloat16 [2048, 16, 128], P(None, 'kv', 'tp'), may hold values from -0.125 to 0.125
- strength_weight: bfloat16 [2048, 16], P(None, 'kv'), may hold values from -0.125 to 0.125
- decay_weight: bfloat16 [2048, 16], P(None, 'kv'), may hold values from -0.125 to 0.125
- head_decay_rate: float32 [16], P('kv'), may hold values from 0.005 to 1.5
- proposal_log_decay: float32 [256, 4, 16], P(None, None, 'kv'), may hold values from -0.69 to 0
- head_norm_gain: bfloat16 [128], P('tp'), may hold values from 0.099609375 to 1.8984375
- output_weight: bfloat16 [16, 128, 2048], P('kv', 'tp'), may hold values from -1.14904852 to 1.14904852
- output_norm_gain: bfloat16 [2048], P(('kv', 'tp')), may hold values from 0.099609375 to 1.8984375
- state: float32 [256, 16, 128, 128], P(None, 'kv', 'tp'), may hold values from -4.5961941 to 4.5961941
- previous_keys: bfloat16 [256, 4, 2048], P(None, None, 'kv'), may hold values from -6 to 6
- previous_values: bfloat16 [256, 4, 16, 128], P(None, None, 'kv', 'tp'), may hold values from -52 to 52
- previous_log_decay: float32 [256, 4, 16], P(None, None, 'kv'), may hold values from -0.7 to -0.02
- previous_strengths: float32 [256, 4, 16], P(None, None, 'kv'), may hold values from 0.1 to 0.9
- accepted: int32 [256], replicated, may hold values from 0 to 4
- parent: int32 [256, 4], replicated, may hold values from -1 to 2, as said below
Outputs:
- layer_out: bfloat16 [256, 4, 2048], P(None, None, ('kv', 'tp'))
- accepted_state: float32 [256, 16, 128, 128], P(None, 'kv', 'tp')
Inputs may be any that keep to these rules, and one draw needn't show every extreme that they name: parent[b, i] is -1 or a proposal index below i; -1 means that proposal i follows the accepted old proposals directly.
All inputs are finite; a program needn't handle non-finite values.
Results may differ from a plain program's by a relative error of at most 0.019.
Values may be sent and summed in bfloat16 or wider, within the bound.
A program may use at most 128 MiB of HBM per device.

v0:
```python
import jax
import jax.numpy as jnp
from jax import lax
from jax.sharding import PartitionSpec as P

epsilon = 1e-06


def unit_rows(matrix):
    return matrix * lax.rsqrt(jnp.sum(matrix * matrix, axis=-1, keepdims=True) + epsilon)


def exact_product(form, left, right):
    return jnp.einsum(form, left, right, precision=lax.Precision.HIGHEST)


def visibility(parent):
    sequence_count, proposal_count = parent.shape
    position = jnp.arange(proposal_count, dtype=jnp.int32)
    parent_hot = (parent[:, :, None] == position[None, None, :]).astype(jnp.float32)
    ancestry = []
    for row_index in range(proposal_count):
        ancestor_row = parent_hot[:, row_index, :]
        if row_index > 0:
            earlier = jnp.stack(ancestry, axis=1)
            ancestor_row = ancestor_row + exact_product(
                "bj,bjk->bk", parent_hot[:, row_index, :row_index], earlier
            )
        ancestry.append(ancestor_row)
    ancestor = jnp.stack(ancestry, axis=1)
    chain = (position[:, None] > position[None, :]).astype(jnp.float32)
    upper = jnp.concatenate(
        [
            jnp.broadcast_to(chain, (sequence_count, proposal_count, proposal_count)),
            jnp.zeros((sequence_count, proposal_count, proposal_count), jnp.float32),
        ],
        axis=2,
    )
    lower = jnp.concatenate(
        [jnp.ones((sequence_count, proposal_count, proposal_count), jnp.float32), ancestor], axis=2
    )
    return jnp.concatenate([upper, lower], axis=1)


def split_heads(matrix, sequence_count, proposal_count, number_of_heads):
    return (
        matrix.astype(jnp.float32)
        .reshape(sequence_count, proposal_count, number_of_heads, -1)
        .transpose(0, 2, 1, 3)
    )


def delta_recursion(
    query_projected,
    key_projected,
    value_projected,
    output_gate_logits,
    write_strength_logits,
    decay_logits,
    decay_speed,
    proposal_group,
    head_norm_gain,
    state,
    previous_keys,
    previous_values,
    previous_log_decay,
    previous_strengths,
    accepted,
    parent,
    channel_count_total,
):
    sequence_count, number_of_heads, value_dim, head_dim = state.shape
    proposal_count = parent.shape[1]
    queries = unit_rows(
        split_heads(query_projected, sequence_count, proposal_count, number_of_heads)
    ) * head_dim ** (-0.5)
    new_keys = unit_rows(
        split_heads(key_projected, sequence_count, proposal_count, number_of_heads)
    )
    old_keys = unit_rows(
        split_heads(previous_keys, sequence_count, proposal_count, number_of_heads)
    )
    new_values = split_heads(value_projected, sequence_count, proposal_count, number_of_heads)
    old_values = split_heads(previous_values, sequence_count, proposal_count, number_of_heads)
    zgate = split_heads(output_gate_logits, sequence_count, proposal_count, number_of_heads)
    beta_new = jax.nn.sigmoid(
        write_strength_logits.reshape(sequence_count, proposal_count, number_of_heads)
    ).transpose(0, 2, 1)
    fresh_decay = (
        -decay_speed[None, None, :]
        * jax.nn.softplus(decay_logits.reshape(sequence_count, proposal_count, number_of_heads))
        + proposal_group
    ).transpose(0, 2, 1)
    position = jnp.arange(proposal_count, dtype=jnp.int32)
    live = (position[None, :] < accepted[:, None]).astype(jnp.float32)[:, None, :]
    beta_old = previous_strengths.transpose(0, 2, 1) * live
    decay_old = previous_log_decay.transpose(0, 2, 1) * live
    keys_all = jnp.concatenate([old_keys, new_keys], axis=2)
    values_all = jnp.concatenate([old_values, new_values], axis=2)
    beta_all = jnp.concatenate([beta_old, beta_new], axis=2)
    decay_all = jnp.concatenate([decay_old, fresh_decay], axis=2)
    visible = visibility(parent)
    gamma_sum = decay_all + exact_product("bij,bhj->bhi", visible, decay_all)
    gamma_diff = gamma_sum[:, :, :, None] - gamma_sum[:, :, None, :]
    decay_pair = jnp.exp(jnp.minimum(gamma_diff, 0.0)) * visible[:, None]
    coupling = (
        beta_all[..., None] * exact_product("bhid,bhjd->bhij", keys_all, keys_all) * decay_pair
    )
    right_side = jnp.concatenate(
        [beta_all[..., None] * values_all, (beta_all * jnp.exp(gamma_sum))[..., None] * keys_all],
        axis=-1,
    )
    solved = []
    for row_index in range(2 * proposal_count):
        current = right_side[:, :, row_index]
        if row_index > 0:
            current = current - exact_product(
                "bhj,bhjd->bhd", coupling[:, :, row_index, :row_index], jnp.stack(solved, axis=2)
            )
        solved.append(current)
    solution = jnp.stack(solved, axis=2)
    update = solution[..., :value_dim] - exact_product(
        "bhcd,bhed->bhce", solution[..., value_dim:], state
    )
    identity = jnp.eye(2 * proposal_count, dtype=jnp.float32)
    seen = visible[:, proposal_count:] + identity[proposal_count:][None]
    reach = jnp.exp(jnp.minimum(gamma_diff[:, :, proposal_count:], 0.0)) * seen[:, None]
    query_key = exact_product("bhid,bhjd->bhij", queries, keys_all) * reach
    readout = exact_product(
        "bhid,bhed->bhie", queries * jnp.exp(gamma_sum[:, :, proposal_count:])[..., None], state
    )
    readout = readout + exact_product("bhij,bhje->bhie", query_key, update)
    squares = channel_count_total(jnp.sum(readout * readout, axis=-1))
    readout = readout * lax.rsqrt(squares / head_dim + epsilon)[..., None]
    readout = readout * head_norm_gain.astype(jnp.float32) * jax.nn.silu(zgate)
    blended_rows = readout.transpose(0, 2, 1, 3).reshape(
        sequence_count * proposal_count, number_of_heads * value_dim
    )
    blended_rows = blended_rows.astype(jnp.bfloat16)
    last_gamma = gamma_sum[:, :, proposal_count - 1 : proposal_count]
    key_weighted = old_keys * jnp.exp(last_gamma - gamma_sum[:, :, :proposal_count])[..., None]
    accepted_state = jnp.exp(last_gamma)[..., None] * state + exact_product(
        "bhcd,bhce->bhed", key_weighted, update[:, :, :proposal_count]
    )
    return (blended_rows, accepted_state)


def channel_sum(squares):
    return lax.psum(squares, "tp")


def on_device(
    tokens,
    input_norm_gain,
    query_weight,
    key_weight,
    value_weight,
    output_gate_weight,
    strength_weight,
    decay_weight,
    head_decay_rate,
    proposal_log_decay,
    head_norm_gain,
    output_weight,
    output_norm_gain,
    state,
    previous_keys,
    previous_values,
    previous_log_decay,
    previous_strengths,
    accepted,
    parent,
):
    gathered = lax.all_gather(tokens, ("kv", "tp"), axis=2, tiled=True)
    sequence_count, proposal_count, width = gathered.shape
    row_total = sequence_count * proposal_count
    features = gathered.astype(jnp.float32)
    normed = features * lax.rsqrt(jnp.mean(features * features, axis=-1, keepdims=True) + epsilon)
    normed = (normed * input_norm_gain.astype(jnp.float32)).astype(jnp.bfloat16)
    flat_rows = normed.reshape(row_total, width)
    write_strength_logits = jnp.dot(flat_rows, strength_weight, preferred_element_type=jnp.float32)
    decay_logits = jnp.dot(flat_rows, decay_weight, preferred_element_type=jnp.float32)
    value_projected = jnp.dot(
        flat_rows, value_weight.reshape(width, -1), preferred_element_type=jnp.float32
    ).astype(jnp.bfloat16)
    output_gate_logits = jnp.dot(
        flat_rows, output_gate_weight.reshape(width, -1), preferred_element_type=jnp.float32
    ).astype(jnp.bfloat16)
    query_projected = jnp.dot(flat_rows, query_weight, preferred_element_type=jnp.float32).astype(
        jnp.bfloat16
    )
    key_projected = jnp.dot(flat_rows, key_weight, preferred_element_type=jnp.float32).astype(
        jnp.bfloat16
    )
    blended_rows, accepted_state = delta_recursion(
        query_projected,
        key_projected,
        value_projected,
        output_gate_logits,
        write_strength_logits,
        decay_logits,
        head_decay_rate,
        proposal_log_decay,
        head_norm_gain,
        state,
        previous_keys,
        previous_values,
        previous_log_decay,
        previous_strengths,
        accepted,
        parent,
        channel_sum,
    )
    partial_out = jnp.dot(
        blended_rows, output_weight.reshape(-1, width), preferred_element_type=jnp.float32
    )
    own_cols = output_norm_gain.shape[0]
    totals = lax.psum(partial_out, ("kv", "tp"))
    scaling = lax.rsqrt(jnp.mean(totals * totals, axis=-1, keepdims=True) + epsilon)
    own_index = lax.axis_index("kv") * lax.axis_size("tp") + lax.axis_index("tp")
    share = lax.dynamic_slice_in_dim(totals, own_index * own_cols, own_cols, 1)
    layer_out = (share * scaling * output_norm_gain.astype(jnp.float32)).astype(jnp.bfloat16)
    return (layer_out.reshape(sequence_count, proposal_count, own_cols), accepted_state)


def solution(mesh):
    placed = (
        P(None, None, ("kv", "tp")),
        P(),
        P(None, "kv"),
        P(None, "kv"),
        P(None, "kv", "tp"),
        P(None, "kv", "tp"),
        P(None, "kv"),
        P(None, "kv"),
        P("kv"),
        P(None, None, "kv"),
        P("tp"),
        P("kv", "tp", None),
        P(("kv", "tp")),
        P(None, "kv", "tp", None),
        P(None, None, "kv"),
        P(None, None, "kv", "tp"),
        P(None, None, "kv"),
        P(None, None, "kv"),
        P(),
        P(),
    )
    return jax.shard_map(
        on_device,
        mesh=mesh,
        in_specs=placed,
        out_specs=(P(None, None, ("kv", "tp")), P(None, "kv", "tp", None)),
        check_vma=False,
    )
```

profile of v0, /device:TPU:0, one launch (start us, length us, event | category | flops | bytes accessed | tf_op | source)
XLA Modules:
  0.0 489.5 jit_solution(4462959712660813374)
XLA Ops:
  17.7 58.3 %all-gather.2.cloned.1.call-done = bf16[256,4,2048]{0,2,1:T(8,128)(2,1)} async-done(((bf16[256,4,64]{0,2,1:T(8,128)(2,1)}), bf16[256,4,2048]{0,2,1:T(8,128)(2,1)}) %all-gather.2.cloned.1.call-update) | async-done | bytes 4194320 | tf_op jit(solution)/shard_map/all_gather | solution.py:174
  76.1 3.2 fusion
  79.5 2.7 fusion.2
  82.2 7.9 %copy.594 = bf16[256,4,2048]{2,1,0:T(4,128)(2,1)} copy(bf16[256,4,2048]{0,2,1:T(8,128)(2,1)} %fusion.2) | data formatting | bytes 8388608 | tf_op jit(solution)/shard_map/convert_element_type | solution.py:179
  90.2 3.0 fusion.61
  98.4 6.9 %reshape.134 = bf16[1024,2048]{1,0:T(8,128)(2,1)} reshape(bf16[256,4,2048]{2,1,0:T(4,128)(2,1)} %copy.594) | data formatting | bytes 8388608 | tf_op jit(solution)/shard_map/reshape | solution.py:180
  105.2 3.4 fusion.9
  115.3 5.3 %multiply_multiply_fusion = f32[256,2,8,8]{3,2,1,0:T(8,128)S(1)} fusion(f32[256,2,4,128]{3,2,1,0:T(4,128)S(1)} %bitcast_multiply_fusion, f32[256,2,4,128]{3,2,1,0:T(4,128)S(1)} %fusion.16, f32[256,8,8]{2,1,0:T(8,128)S(1)} %copy-done.22, f32[256,2,8]{2,1,0:T(2,128)} %copy.621, f32[256,2,8]{2,1,0:T(2,128)S(1)} %copy.615), kind=kOutput, calls=%fused_computation.26 | convolution fusion | flops 51019776 | bytes 2326528 | tf_op jit(solution)/shard_map/bhid,bhjd->bhij/dot_general | solution.py:14
  128.1 3.4 fusion.10
  133.5 15.6 %fusion.22 = f32[256,2,4,32]{3,2,1,0:T(4,128)S(1)} fusion(f32[256,2,32,128]{3,2,1,0:T(8,128)} %param.33, f32[256,4,2,128]{3,2,1,0:T(2,128)S(1)} %reshape.152, f32[256,2,4]{2,1,0:T(2,128)S(1)} %copy.609, f32[256,2,4]{2,1,0:T(2,128)S(1)} %copy.597), kind=kOutput, calls=%fused_computation.58 | convolution fusion | flops 101187584 | bytes 9715712 | tf_op jit(solution)/shard_map/bhid,bhed->bhie/dot_general | solution.py:14
  157.2 10.5 %pad_maximum_fusion.7 = (f32[256,2,1,160]{3,2,1,0:T(1,128)}, f32[256,2,1,160]{3,2,1,0:T(1,128)S(1)}, f32[256,2,1,160]{3,2,1,0:T(1,128)S(1)}, f32[256,2,1,160]{3,...) fusion(f32[256,2,8,128]{3,2,1,0:T(8,128)S(1)} %fusion.8, ...), kind=kLoop, calls=%fused_computation.72 | loop fusion | flops 655360 | bytes 5242880 | tf_op jit(solution)/shard_map/concatenate | solution.py:109
  170.8 7.6 %fusion.24 = f32[256,2,1,160]{3,2,1,0:T(1,128)} fusion(f32[256,2,1,160]{3,2,1,0:T(1,128)S(1)} %copy.650, f32[256,2,1,160]{3,2,1,0:T(1,128)S(1)} %get-tuple-element.41, f32[256,2,8,8]{3,2,1,0:T(8,128)} %copy-done.6), kind=kOutput, calls=%fused_computation.60 | convolution fusion | flops 2129920 | bytes 1245184 | tf_op jit(solution)/shard_map/bhj,bhjd->bhd/dot_general | solution.py:14
  188.9 8.4 %fusion.5 = f32[256,2,1,160]{3,2,1,0:T(1,128)} fusion(f32[256,2,1,160]{3,2,1,0:T(1,128)} %copy.652, f32[256,2,1,160]{3,2,1,0:T(1,128)} %copy.651, f32[256,2,1,160]{3,2,1,0:T(1,128)} %copy-done.8, f32[256,2,1,160]{3,2,1,0:T(1,128)S(1)} %get-tuple-element.41, f32[256,2,8,8]{3,2,1,0:T(8,128)S(1)} %copy-done.7), kind=kOutput, calls=%fused_computation.28 | convolution fusion | flops 4915200 | bytes 2097152 | tf_op jit(solution)/shard_map/bhj,bhjd->bhd/dot_general | solution.py:14
  220.7 11.4 %stack.101 = f32[256,2,7,160]{3,2,1,0:T(8,128)} concatenate(f32[256,2,1,160]{3,2,1,0:T(1,128)S(1)} %get-tuple-element.41, f32[256,2,1,160]{3,2,1,0:T(1,128)S(1)} %copy-done.9, f32[256,2,1,160]{3,2,1,0:T(1,128)} %copy.651, f32[256,2,1,160]{3,2,1,0:T(1,128)} %copy.652, f32[256,2,1,160]{3,2,1,0:T(1,128)} %copy.653, f32[256,2,1,160]{3,2,1,0:T(1,128)} %copy.654, f32[256,2,1,160]{3,2,1,0:T(1,128)} %copy.655), dimensions={2} | concatenate | bytes 4587520 | tf_op jit(solution)/shard_map/stack | solution.py:118
  232.2 7.2 %fusion.48 = f32[256,2,1,160]{3,2,1,0:T(1,128)} fusion(f32[256,2,7,160]{3,2,1,0:T(8,128)} %stack.101, f32[256,2,8,8]{3,2,1,0:T(8,128)S(1)} %copy-done.7), kind=kOutput, calls=%fused_computation.96 | convolution fusion | flops 6881280 | bytes 2883584 | tf_op jit(solution)/shard_map/bhj,bhjd->bhd/dot_general | solution.py:14
  246.2 11.2 %stack.103 = f32[256,2,8,160]{3,2,1,0:T(8,128)} concatenate(f32[256,2,1,160]{3,2,1,0:T(1,128)S(1)} %get-tuple-element.41, f32[256,2,1,160]{3,2,1,0:T(1,128)S(1)} %copy-done.9, f32[256,2,1,160]{3,2,1,0:T(1,128)S(1)} %copy-done.10, f32[256,2,1,160]{3,2,1,0:T(1,128)S(1)} %copy-done.11, f32[256,2,1,160]{3,2,1,0:T(1,128)S(1)} %copy-done.12, f32[256,2,1,160]{3,2,1,0:T(1,128)S(1)} %copy-done.13, ...), dimensions={2} | concatenate | bytes 5242880 | tf_op jit(solution)/shard_map/stack | solution.py:121
  257.4 16.8 %slice_subtract_fusion = f32[256,2,8,32]{3,2,1,0:T(8,128)S(1)} fusion(f32[256,2,8,160]{3,2,1,0:T(8,128)} %stack.103, f32[256,2,32,128]{3,2,1,0:T(8,128)} %param.33), kind=kOutput, calls=%fused_computation.23 | convolution fusion | flops 201457664 | bytes 11534336 | tf_op jit(solution)/shard_map/bhcd,bhed->bhce/dot_general | solution.py:14
  274.3 4.2 convolution_multiply_fusion
  278.6 3.4 fusion.95
  284.3 6.4 %psum.14 = f32[256,2,4]{0,2,1:T(4,128)S(1)} all-reduce(f32[256,2,4]{0,2,1:T(4,128)S(1)} %copy.659), channel_id=1, replica_groups=mesh['kv'=8,'tp'=4] {'tp'}, use_global_device_ids=true, to_apply=%region_5.6 | all-reduce | flops 2048 | bytes 16384 | tf_op jit(solution)/shard_map/psum | solution.py:149
  292.8 4.5 fusion.96
  298.4 18.9 %multiply_add_fusion = f32[256,2,32,128]{3,2,1,0:T(8,128)} fusion(f32[256,2,32,128]{3,2,1,0:T(8,128)} %param.33, f32[256,2]{1,0:T(8,128)S(1)} %bitcast.222, f32[256,2,8,32]{3,2,1,0:T(8,128)S(1)} %slice_subtract_fusion, f32[256,2,4]{2,1,0:T(2,128)S(1)} %copy.666, bf16[256,4,256]{2,1,0:T(4,128)(2,1)S(1)} %copy-done.26, f32[256,2,4]{2,1,0:T(2,128)S(1)} %copy-done.32), kind=kOutput, calls=%fused_computation.19 | convolution fusion | flops 105644032 | bytes 19005440 | tf_op jit(solution)/shard_map/bhcd,bhce->bhed/dot_general | solution.py:14
  317.2 158.6 %all-reduce.4.cloned.1.call-done = f32[1024,2048]{1,0:T(8,128)} async-done(((f32[1024,2048]{1,0:T(8,128)}), f32[1024,2048]{1,0:T(8,128)}) %all-reduce.4.cloned.1.call-update) | async-done | bytes 8388624 | tf_op jit(solution)/shard_map/psum | solution.py:218
  475.8 4.1 multiply_reduce_fusion
  (226 shorter events, 91.0 us)
Async XLA Ops:
  7.2 98.1 %copy-start = (bf16[2048,256]{1,0:T(8,128)(2,1)S(1)}, bf16[2048,256]{1,0:T(8,128)(2,1)}, u32[]{:S(2)}) copy-start(bf16[2048,256]{1,0:T(8,128)(2,1)} %param.23) | copy-start | bytes 3145732
  7.2 7.7 %copy-start.41 = (bf16[256,4,2,32]{0,3,2,1:T(8,128)(2,1)S(1)}, bf16[256,4,2,32]{0,3,2,1:T(8,128)(2,1)}, u32[]{:S(2)}) copy-start(bf16[256,4,2,32]{0,3,2,1:T(8,128)(2,1)} %param.35) | copy-start | bytes 393220
  7.2 8.8 %copy-start.47 = (s32[256]{0:T(256)S(1)}, s32[256]{0:T(256)}, u32[]{:S(2)}) copy-start(s32[256]{0:T(256)} %param.38) | copy-start | bytes 3076
  7.2 8.8 %copy-start.44 = (f32[256,4,2]{0,2,1:T(2,128)S(1)}, f32[256,4,2]{0,2,1:T(2,128)}, u32[]{:S(2)}) copy-start(f32[256,4,2]{0,2,1:T(2,128)} %param.36) | copy-start | bytes 24580
  7.2 8.8 %copy-start.45 = (f32[256,4,2]{0,2,1:T(2,128)S(1)}, f32[256,4,2]{0,2,1:T(2,128)}, u32[]{:S(2)}) copy-start(f32[256,4,2]{0,2,1:T(2,128)} %param.37) | copy-start | bytes 24580
  7.2 68.8 %all-gather.2.cloned.1.call-start = ((), (), s32[]{:S(2)}) async-start(), calls=%async_computation | async-start | bytes 4325376 | tf_op jit(solution)/shard_map/all_gather | solution.py:174
  8.0 467.8 %all-reduce.4.cloned.1.call-start = ((), (), s32[]{:S(2)}) async-start(), calls=%async_computation.1 | async-start | bytes 16777216 | tf_op jit(solution)/shard_map/psum | solution.py:218
  11.4 83.1 %copy-start.21 = (f32[256,8,8]{2,1,0:T(8,128)}, f32[256,8,8]{2,1,0:T(8,128)S(1)}, u32[]{:S(2)}) copy-start(f32[256,8,8]{2,1,0:T(8,128)S(1)} %copy.607) | copy-start | bytes 196612
  13.9 65.3 %copy-start.31 = (f32[256,2,4]{2,1,0:T(2,128)}, f32[256,2,4]{2,1,0:T(2,128)S(1)}, u32[]{:S(2)}) copy-start(f32[256,2,4]{2,1,0:T(2,128)S(1)} %copy.611) | copy-start | bytes 24580
  17.7 97.6 %copy-start.14 = (f32[256,2,4,128]{3,2,1,0:T(4,128)}, f32[256,2,4,128]{3,2,1,0:T(4,128)S(1)}, u32[]{:S(2)}) copy-start(f32[256,2,4,128]{3,2,1,0:T(4,128)S(1)} %fusion.16) | copy-start | bytes 3145732
  82.2 7.9 %copy-start.42 = (bf16[2048,2]{0,1:T(2,128)(2,1)S(1)}, bf16[2048,2]{0,1:T(2,128)(2,1)}, u32[]{:S(2)}) copy-start(bf16[2048,2]{0,1:T(2,128)(2,1)} %param.27) | copy-start | bytes 24580
  112.8 7.9 %copy-start.17 = (f32[256,2,4,128]{3,2,1,0:T(4,128)}, f32[256,2,4,128]{3,2,1,0:T(4,128)S(1)}, u32[]{:S(2)}) copy-start(f32[256,2,4,128]{3,2,1,0:T(4,128)S(1)} %bitcast_multiply_fusion) | copy-start | bytes 3145732
  115.3 9.1 %copy-start.3 = (bf16[1024,2048]{1,0:T(8,128)(2,1)S(1)}, bf16[1024,2048]{1,0:T(8,128)(2,1)}, u32[]{:S(2)}) copy-start(bf16[1024,2048]{1,0:T(8,128)(2,1)} %reshape.134) | copy-start | bytes 12582916
  133.5 15.6 %copy-start.39 = (f32[256,2,4]{2,1,0:T(2,128)}, f32[256,2,4]{2,1,0:T(2,128)S(1)}, u32[]{:S(2)}) copy-start(f32[256,2,4]{2,1,0:T(2,128)S(1)} %copy.597) | copy-start | bytes 24580
  157.2 11.8 %copy-start.34 = (f32[256,2,1,1]{3,2,1,0:T(1,128)S(1)}, f32[256,2,1,1]{3,2,1,0:T(1,128)}, u32[]{:S(2)}) copy-start(f32[256,2,1,1]{3,2,1,0:T(1,128)} %slice.141) | copy-start | bytes 6148
  170.8 7.6 %copy-start.8 = (f32[256,2,1,160]{3,2,1,0:T(1,128)}, f32[256,2,1,160]{3,2,1,0:T(1,128)S(1)}, u32[]{:S(2)}) copy-start(f32[256,2,1,160]{3,2,1,0:T(1,128)S(1)} %copy.650) | copy-start | bytes 983044
  170.8 8.9 %copy-start.29 = (f32[256,2,1,160]{3,2,1,0:T(1,128)S(1)}, f32[256,2,1,160]{3,2,1,0:T(1,128)}, u32[]{:S(2)}) copy-start(f32[256,2,1,160]{3,2,1,0:T(1,128)} %get-tuple-element.43) | copy-start | bytes 983044
  257.3 16.9 %copy-start.16 = (f32[256,2,4,128]{3,2,1,0:T(4,128)S(1)}, f32[256,2,4,128]{3,2,1,0:T(4,128)}, u32[]{:S(2)}) copy-start(f32[256,2,4,128]{3,2,1,0:T(4,128)} %copy-done.14) | copy-start | bytes 3145732
  257.4 16.9 %copy-start.18 = (f32[256,2,4,128]{3,2,1,0:T(4,128)S(1)}, f32[256,2,4,128]{3,2,1,0:T(4,128)}, u32[]{:S(2)}) copy-start(f32[256,2,4,128]{3,2,1,0:T(4,128)} %copy-done.17) | copy-start | bytes 3145732
  257.4 16.9 %copy-start.20 = (f32[256,4,2,128]{3,2,1,0:T(2,128)S(1)}, f32[256,4,2,128]{3,2,1,0:T(2,128)}, u32[]{:S(2)}) copy-start(f32[256,4,2,128]{3,2,1,0:T(2,128)} %copy-done.19) | copy-start | bytes 3145732
  257.4 16.9 %copy-start.25 = (f32[256,2,8,8]{3,2,1,0:T(8,128)S(1)}, f32[256,2,8,8]{3,2,1,0:T(8,128)}, u32[]{:S(2)}) copy-start(f32[256,2,8,8]{3,2,1,0:T(8,128)} %broadcast_subtract_fusion) | copy-start | bytes 393220
  257.4 16.9 %copy-start.35 = (f32[256,4,8]{2,1,0:T(4,128)S(1)}, f32[256,4,8]{2,1,0:T(4,128)}, u32[]{:S(2)}) copy-start(f32[256,4,8]{2,1,0:T(4,128)} %copy.617) | copy-start | bytes 98308
  257.4 16.9 %copy-start.40 = (f32[256,2,4]{2,1,0:T(2,128)S(1)}, f32[256,2,4]{2,1,0:T(2,128)}, u32[]{:S(2)}) copy-start(f32[256,2,4]{2,1,0:T(2,128)} %copy-done.39) | copy-start | bytes 24580
  283.2 9.6 %copy-start.38 = (bf16[2,32,2048]{2,1,0:T(8,128)(2,1)S(1)}, bf16[2,32,2048]{2,1,0:T(8,128)(2,1)}, u32[]{:S(2)}) copy-start(bf16[2,32,2048]{2,1,0:T(8,128)(2,1)} %param.31) | copy-start | bytes 786436
  (28 other events, 99.4 us)
Sparse Core Ops, SparseCore 0:
  10.9 65.0 all-gather.1
  297.4 178.3 all-reduce.3
where the time goes:
time: 496 us; the launch traced here: 489 us
  waiting for transfers between devices  218 us (44%)
  matrix products  108 us (22%)
  local copies, waits for them, and re-layouts  89.5 us (18%)
  other arithmetic  52.6 us (11%)
  between operations  15.5 us (3%)
  blocking collectives  6.36 us (1%)
    psum x1, waiting for transfers between devices, on_device(): totals = lax.psum(partial_out, ('kv', 'tp'))  159 us
    dot_general x10, matrix products, exact_product(): return jnp.einsum(form, left, right, precision=lax.Precision.HIGHEST)  90 us
    all_gather x1, waiting for transfers between devices, on_device(): gathered = lax.all_gather(tokens, ('kv', 'tp'), axis=2, tiled=True)  58.3 us
    another operation x8, local copies, waits for them, and re-layouts, delta_recursion(): solution = jnp.stack(solved, axis=2)  22.3 us
    another operation x2, local copies, waits for them, and re-layouts, delta_recursion(): jnp.stack(solved, axis=2)  12.1 us
    unnamed x110, local copies, waits for them, and re-layouts  11 us
    concatenate x1, other arithmetic, delta_recursion(): jnp.concatenate([beta_all[..., None] * values_all, (beta_all * jnp.exp(ga...  10.5 us
  transfers between devices with their start and end apart: 2, of which 2 were waited for; matrix products, arithmetic and copies ran while one was open for 6% of the time, Pallas kernels for 0%

commit v1 on v0

--- a/solution.py
+++ b/solution.py
@@ -215,7 +215,7 @@
         blended_rows, output_weight.reshape(-1, width), preferred_element_type=jnp.float32
     )
     own_cols = output_norm_gain.shape[0]
-    totals = lax.psum(partial_out, ("kv", "tp"))
+    totals = lax.psum(lax.psum(partial_out, "kv"), "tp")
     scaling = lax.rsqrt(jnp.mean(totals * totals, axis=-1, keepdims=True) + epsilon)
     own_index = lax.axis_index("kv") * lax.axis_size("tp") + lax.axis_index("tp")
     share = lax.dynamic_slice_in_dim(totals, own_index * own_cols, own_cols, 1)

time: 496 us -> 741 us (1.49)
  waiting for transfers between devices: 218 us -> 463 us
    psum x1 -> x2, waiting for transfers between devices: 159 us -> 404 us  [on_device(): totals = lax.psum(lax.psum(partial_out, 'kv'), 'tp')]
  transfers between devices with their start and end apart: 2 -> 3, of which waited for: 2 -> 3; matrix products, arithmetic and copies ran while one was open for 6% -> 4% of each run, Pallas kernels for 0% -> 0%
where the time goes in v1:
time: 741 us; the launch traced here: 734 us
  waiting for transfers between devices  463 us (62%)
  matrix products  108 us (15%)
  local copies, waits for them, and re-layouts  89.2 us (12%)
  other arithmetic  52.6 us (7%)
  between operations  15.2 us (2%)
    psum x2, waiting for transfers between devices, on_device(): totals = lax.psum(lax.psum(partial_out, 'kv'), 'tp')  404 us
    dot_general x10, matrix products, exact_product(): return jnp.einsum(form, left, right, precision=lax.Precision.HIGHEST)  90.3 us
    all_gather x1, waiting for transfers between devices, on_device(): gathered = lax.all_gather(tokens, ('kv', 'tp'), axis=2, tiled=True)  58.3 us
    another operation x8, local copies, waits for them, and re-layouts, delta_recursion(): solution = jnp.stack(solved, axis=2)  22.3 us
  transfers between devices with their start and end apart: 3, of which 3 were waited for; matrix products, arithmetic and copies ran while one was open for 4% of the time, Pallas kernels for 0%

profile of v1, /device:TPU:0, one launch (start us, length us, event | category | flops | bytes accessed | tf_op | source)
XLA Modules:
  0.0 734.5 jit_solution(16359781349255441863)
XLA Ops:
  17.7 58.3 %all-gather.2.cloned.1.call-done = bf16[256,4,2048]{0,2,1:T(8,128)(2,1)} async-done(((bf16[256,4,64]{0,2,1:T(8,128)(2,1)}), bf16[256,4,2048]{0,2,1:T(8,128)(2,1)}) %all-gather.2.cloned.1.call-update) | async-done | bytes 4194320 | tf_op jit(solution)/shard_map/all_gather | solution.py:174
  76.1 3.2 fusion
  82.2 7.9 %copy.594 = bf16[256,4,2048]{2,1,0:T(4,128)(2,1)} copy(bf16[256,4,2048]{0,2,1:T(8,128)(2,1)} %fusion.2) | data formatting | bytes 8388608 | tf_op jit(solution)/shard_map/convert_element_type | solution.py:179
  90.2 3.0 fusion.61
  98.4 6.9 reshape.134
  105.2 3.4 fusion.9
  115.3 5.3 multiply_multiply_fusion
  128.1 3.4 fusion.10
  133.5 15.6 %fusion.22 = f32[256,2,4,32]{3,2,1,0:T(4,128)S(1)} fusion(f32[256,2,32,128]{3,2,1,0:T(8,128)} %param.33, f32[256,4,2,128]{3,2,1,0:T(2,128)S(1)} %reshape.152, f32[256,2,4]{2,1,0:T(2,128)S(1)} %copy.609, f32[256,2,4]{2,1,0:T(2,128)S(1)} %copy.597), kind=kOutput, calls=%fused_computation.58 | convolution fusion | flops 101187584 | bytes 9715712 | tf_op jit(solution)/shard_map/bhid,bhed->bhie/dot_general | solution.py:14
  157.2 10.5 %pad_maximum_fusion.7 = (f32[256,2,1,160]{3,2,1,0:T(1,128)}, f32[256,2,1,160]{3,2,1,0:T(1,128)S(1)}, f32[256,2,1,160]{3,2,1,0:T(1,128)S(1)}, f32[256,2,1,160]{3,...) fusion(f32[256,2,8,128]{3,2,1,0:T(8,128)S(1)} %fusion.8, ...), kind=kLoop, calls=%fused_computation.72 | loop fusion | flops 655360 | bytes 5242880 | tf_op jit(solution)/shard_map/concatenate | solution.py:109
  170.8 7.6 %fusion.24 = f32[256,2,1,160]{3,2,1,0:T(1,128)} fusion(f32[256,2,1,160]{3,2,1,0:T(1,128)S(1)} %copy.650, f32[256,2,1,160]{3,2,1,0:T(1,128)S(1)} %get-tuple-element.41, f32[256,2,8,8]{3,2,1,0:T(8,128)} %copy-done.6), kind=kOutput, calls=%fused_computation.60 | convolution fusion | flops 2129920 | bytes 1245184 | tf_op jit(solution)/shard_map/bhj,bhjd->bhd/dot_general | solution.py:14
  188.9 8.4 %fusion.5 = f32[256,2,1,160]{3,2,1,0:T(1,128)} fusion(f32[256,2,1,160]{3,2,1,0:T(1,128)} %copy.652, f32[256,2,1,160]{3,2,1,0:T(1,128)} %copy.651, f32[256,2,1,160]{3,2,1,0:T(1,128)} %copy-done.8, f32[256,2,1,160]{3,2,1,0:T(1,128)S(1)} %get-tuple-element.41, f32[256,2,8,8]{3,2,1,0:T(8,128)S(1)} %copy-done.7), kind=kOutput, calls=%fused_computation.28 | convolution fusion | flops 4915200 | bytes 2097152 | tf_op jit(solution)/shard_map/bhj,bhjd->bhd/dot_general | solution.py:14
  220.7 11.4 %stack.101 = f32[256,2,7,160]{3,2,1,0:T(8,128)} concatenate(f32[256,2,1,160]{3,2,1,0:T(1,128)S(1)} %get-tuple-element.41, f32[256,2,1,160]{3,2,1,0:T(1,128)S(1)} %copy-done.9, f32[256,2,1,160]{3,2,1,0:T(1,128)} %copy.651, f32[256,2,1,160]{3,2,1,0:T(1,128)} %copy.652, f32[256,2,1,160]{3,2,1,0:T(1,128)} %copy.653, f32[256,2,1,160]{3,2,1,0:T(1,128)} %copy.654, f32[256,2,1,160]{3,2,1,0:T(1,128)} %copy.655), dimensions={2} | concatenate | bytes 4587520 | tf_op jit(solution)/shard_map/stack | solution.py:118
  232.2 7.2 fusion.48
  246.2 11.2 %stack.103 = f32[256,2,8,160]{3,2,1,0:T(8,128)} concatenate(f32[256,2,1,160]{3,2,1,0:T(1,128)S(1)} %get-tuple-element.41, f32[256,2,1,160]{3,2,1,0:T(1,128)S(1)} %copy-done.9, f32[256,2,1,160]{3,2,1,0:T(1,128)S(1)} %copy-done.10, f32[256,2,1,160]{3,2,1,0:T(1,128)S(1)} %copy-done.11, f32[256,2,1,160]{3,2,1,0:T(1,128)S(1)} %copy-done.12, f32[256,2,1,160]{3,2,1,0:T(1,128)S(1)} %copy-done.13, ...), dimensions={2} | concatenate | bytes 5242880 | tf_op jit(solution)/shard_map/stack | solution.py:121
  257.4 16.8 %slice_subtract_fusion = f32[256,2,8,32]{3,2,1,0:T(8,128)S(1)} fusion(f32[256,2,8,160]{3,2,1,0:T(8,128)} %stack.103, f32[256,2,32,128]{3,2,1,0:T(8,128)} %param.33), kind=kOutput, calls=%fused_computation.23 | convolution fusion | flops 201457664 | bytes 11534336 | tf_op jit(solution)/shard_map/bhcd,bhed->bhce/dot_general | solution.py:14
  274.3 4.2 convolution_multiply_fusion
  278.6 3.4 fusion.95
  284.3 6.4 psum.21
  292.5 4.6 fusion.96
  297.2 269.5 %all-reduce.5.cloned.1.call-done = f32[1024,2048]{1,0:T(8,128)} async-done(((f32[1024,2048]{1,0:T(8,128)}), f32[1024,2048]{1,0:T(8,128)}) %all-reduce.5.cloned.1.call-update) | async-done | bytes 8388624 | tf_op jit(solution)/shard_map/psum | solution.py:218
  567.8 19.1 %multiply_add_fusion = f32[256,2,32,128]{3,2,1,0:T(8,128)} fusion(f32[256,2,32,128]{3,2,1,0:T(8,128)} %param.33, f32[256,2]{1,0:T(8,128)S(1)} %bitcast.222, f32[256,2,8,32]{3,2,1,0:T(8,128)S(1)} %slice_subtract_fusion, f32[256,2,4]{2,1,0:T(2,128)S(1)} %copy.666, bf16[256,4,256]{2,1,0:T(4,128)(2,1)S(1)} %copy-done.26, f32[256,2,4]{2,1,0:T(2,128)S(1)} %copy-done.32), kind=kOutput, calls=%fused_computation.19 | convolution fusion | flops 105644032 | bytes 19005440 | tf_op jit(solution)/shard_map/bhcd,bhce->bhed/dot_general | solution.py:14
  586.9 134.2 %all-reduce.7.cloned.1.call-done = f32[1024,2048]{1,0:T(8,128)} async-done(((f32[1024,2048]{1,0:T(8,128)}), f32[1024,2048]{1,0:T(8,128)}) %all-reduce.7.cloned.1.call-update) | async-done | bytes 8388624 | tf_op jit(solution)/shard_map/psum | solution.py:218
  721.1 4.1 multiply_reduce_fusion
  (229 shorter events, 93.5 us)
Async XLA Ops:
  7.2 98.1 %copy-start = (bf16[2048,256]{1,0:T(8,128)(2,1)S(1)}, bf16[2048,256]{1,0:T(8,128)(2,1)}, u32[]{:S(2)}) copy-start(bf16[2048,256]{1,0:T(8,128)(2,1)} %param.23) | copy-start | bytes 3145732
  7.2 7.7 %copy-start.41 = (bf16[256,4,2,32]{0,3,2,1:T(8,128)(2,1)S(1)}, bf16[256,4,2,32]{0,3,2,1:T(8,128)(2,1)}, u32[]{:S(2)}) copy-start(bf16[256,4,2,32]{0,3,2,1:T(8,128)(2,1)} %param.35) | copy-start | bytes 393220
  7.2 8.8 %copy-start.47 = (s32[256]{0:T(256)S(1)}, s32[256]{0:T(256)}, u32[]{:S(2)}) copy-start(s32[256]{0:T(256)} %param.38) | copy-start | bytes 3076
  7.2 8.8 %copy-start.44 = (f32[256,4,2]{0,2,1:T(2,128)S(1)}, f32[256,4,2]{0,2,1:T(2,128)}, u32[]{:S(2)}) copy-start(f32[256,4,2]{0,2,1:T(2,128)} %param.36) | copy-start | bytes 24580
  7.2 8.8 %copy-start.45 = (f32[256,4,2]{0,2,1:T(2,128)S(1)}, f32[256,4,2]{0,2,1:T(2,128)}, u32[]{:S(2)}) copy-start(f32[256,4,2]{0,2,1:T(2,128)} %param.37) | copy-start | bytes 24580
  7.2 68.8 %all-gather.2.cloned.1.call-start = ((), (), s32[]{:S(2)}) async-start(), calls=%async_computation | async-start | bytes 4325376 | tf_op jit(solution)/shard_map/all_gather | solution.py:174
  8.0 558.7 %all-reduce.5.cloned.1.call-start = ((), (), s32[]{:S(2)}) async-start(), calls=%async_computation.1 | async-start | bytes 16777216 | tf_op jit(solution)/shard_map/psum | solution.py:218
  11.4 83.1 %copy-start.21 = (f32[256,8,8]{2,1,0:T(8,128)}, f32[256,8,8]{2,1,0:T(8,128)S(1)}, u32[]{:S(2)}) copy-start(f32[256,8,8]{2,1,0:T(8,128)S(1)} %copy.607) | copy-start | bytes 196612
  13.9 65.3 %copy-start.31 = (f32[256,2,4]{2,1,0:T(2,128)}, f32[256,2,4]{2,1,0:T(2,128)S(1)}, u32[]{:S(2)}) copy-start(f32[256,2,4]{2,1,0:T(2,128)S(1)} %copy.611) | copy-start | bytes 24580
  17.7 97.6 %copy-start.14 = (f32[256,2,4,128]{3,2,1,0:T(4,128)}, f32[256,2,4,128]{3,2,1,0:T(4,128)S(1)}, u32[]{:S(2)}) copy-start(f32[256,2,4,128]{3,2,1,0:T(4,128)S(1)} %fusion.16) | copy-start | bytes 3145732
  82.2 7.9 %copy-start.42 = (bf16[2048,2]{0,1:T(2,128)(2,1)S(1)}, bf16[2048,2]{0,1:T(2,128)(2,1)}, u32[]{:S(2)}) copy-start(bf16[2048,2]{0,1:T(2,128)(2,1)} %param.27) | copy-start | bytes 24580
  112.8 7.9 %copy-start.17 = (f32[256,2,4,128]{3,2,1,0:T(4,128)}, f32[256,2,4,128]{3,2,1,0:T(4,128)S(1)}, u32[]{:S(2)}) copy-start(f32[256,2,4,128]{3,2,1,0:T(4,128)S(1)} %bitcast_multiply_fusion) | copy-start | bytes 3145732
  115.3 9.1 %copy-start.3 = (bf16[1024,2048]{1,0:T(8,128)(2,1)S(1)}, bf16[1024,2048]{1,0:T(8,128)(2,1)}, u32[]{:S(2)}) copy-start(bf16[1024,2048]{1,0:T(8,128)(2,1)} %reshape.134) | copy-start | bytes 12582916
  133.5 15.6 %copy-start.39 = (f32[256,2,4]{2,1,0:T(2,128)}, f32[256,2,4]{2,1,0:T(2,128)S(1)}, u32[]{:S(2)}) copy-start(f32[256,2,4]{2,1,0:T(2,128)S(1)} %copy.597) | copy-start | bytes 24580
  157.2 11.8 %copy-start.34 = (f32[256,2,1,1]{3,2,1,0:T(1,128)S(1)}, f32[256,2,1,1]{3,2,1,0:T(1,128)}, u32[]{:S(2)}) copy-start(f32[256,2,1,1]{3,2,1,0:T(1,128)} %slice.141) | copy-start | bytes 6148
  170.8 8.9 %copy-start.29 = (f32[256,2,1,160]{3,2,1,0:T(1,128)S(1)}, f32[256,2,1,160]{3,2,1,0:T(1,128)}, u32[]{:S(2)}) copy-start(f32[256,2,1,160]{3,2,1,0:T(1,128)} %get-tuple-element.43) | copy-start | bytes 983044
  257.3 16.9 %copy-start.16 = (f32[256,2,4,128]{3,2,1,0:T(4,128)S(1)}, f32[256,2,4,128]{3,2,1,0:T(4,128)}, u32[]{:S(2)}) copy-start(f32[256,2,4,128]{3,2,1,0:T(4,128)} %copy-done.14) | copy-start | bytes 3145732
  257.4 16.9 %copy-start.18 = (f32[256,2,4,128]{3,2,1,0:T(4,128)S(1)}, f32[256,2,4,128]{3,2,1,0:T(4,128)}, u32[]{:S(2)}) copy-start(f32[256,2,4,128]{3,2,1,0:T(4,128)} %copy-done.17) | copy-start | bytes 3145732
  257.4 16.9 %copy-start.20 = (f32[256,4,2,128]{3,2,1,0:T(2,128)S(1)}, f32[256,4,2,128]{3,2,1,0:T(2,128)}, u32[]{:S(2)}) copy-start(f32[256,4,2,128]{3,2,1,0:T(2,128)} %copy-done.19) | copy-start | bytes 3145732
  257.4 16.9 %copy-start.25 = (f32[256,2,8,8]{3,2,1,0:T(8,128)S(1)}, f32[256,2,8,8]{3,2,1,0:T(8,128)}, u32[]{:S(2)}) copy-start(f32[256,2,8,8]{3,2,1,0:T(8,128)} %broadcast_subtract_fusion) | copy-start | bytes 393220
  257.4 16.9 %copy-start.35 = (f32[256,4,8]{2,1,0:T(4,128)S(1)}, f32[256,4,8]{2,1,0:T(4,128)}, u32[]{:S(2)}) copy-start(f32[256,4,8]{2,1,0:T(4,128)} %copy.617) | copy-start | bytes 98308
  257.4 16.9 %copy-start.40 = (f32[256,2,4]{2,1,0:T(2,128)S(1)}, f32[256,2,4]{2,1,0:T(2,128)}, u32[]{:S(2)}) copy-start(f32[256,2,4]{2,1,0:T(2,128)} %copy-done.39) | copy-start | bytes 24580
  283.2 9.3 %copy-start.38 = (bf16[2,32,2048]{2,1,0:T(8,128)(2,1)S(1)}, bf16[2,32,2048]{2,1,0:T(8,128)(2,1)}, u32[]{:S(2)}) copy-start(bf16[2,32,2048]{2,1,0:T(8,128)(2,1)} %param.31) | copy-start | bytes 786436
  297.1 424.0 %all-reduce.7.cloned.1.call-start = ((), (), s32[]{:S(2)}) async-start(), calls=%async_computation.2 | async-start | bytes 16777216 | tf_op jit(solution)/shard_map/psum | solution.py:218
  (29 other events, 107.1 us)
Sparse Core Ops, SparseCore 0:
  10.9 65.0 all-gather.1
  297.3 269.3 all-reduce.4
  569.1 151.9 all-reduce.6
